TPU v7x, 32 devices: a whole 2x2x4 slice. The times are simulated.
32 devices in a mesh: ep: 8 (over z, y), tp: 4 (over x, core).
Axes of the slice: x: 2, y: 2, z: 4, core: 2. Of those that a mesh axis runs over, the one named last changes fastest.
Arguments:
- tokens: bfloat16 [2048, 2048], P('ep', 'tp'), may hold values from -72 to 72
- norm_gain: bfloat16 [2048], P('tp'), may hold values from 0.099609375 to 1.8984375
- expert_ids: int32 [2048, 2], P('ep'), may hold values from 0 to 7, all different within a row; in each aligned block of 256 rows (0 to 255, 256 to 511, ...) at most 128 rows name the same one
- gate_share: float32 [2048, 2], P('ep'), may hold values from 0.1 to 1
- gate_weight: bfloat16 [8, 2048, 4096], P('ep', None, 'tp'), may hold values from -0.125 to 0.125
- up_weight: bfloat16 [8, 2048, 4096], P('ep', None, 'tp'), may hold values from -0.125 to 0.125
- down_weight: bfloat16 [8, 4096, 2048], P('ep', 'tp'), may hold values from -0.09375 to 0.09375
Outputs:
- mixed: bfloat16 [2048, 2048], P('ep', 'tp')
Inputs may be any that keep to these rules, and one draw needn't show every extreme that they name: `expert_ids`: each token names two different experts; among the 256 tokens of one index of ep no expert is named more than 128 times, a bound that some block reaches.
All inputs are finite; a program needn't handle non-finite values.
Results may differ from a plain program's by a relative error of at most 0.019.
Values may be sent and summed in bfloat16 or wider, within the bound.
A program may use at most 64 MiB of HBM per device.

v0:
```python
import jax
import jax.numpy as jnp
from jax import lax
from jax.sharding import PartitionSpec as P

D = 2048


EPS = 1e-06


def shards(tokens, norm_gain, expert_ids, gate_share, gate_weight, up_weight, down_weight):
    n_expdev = lax.axis_size("ep")
    exp_local = gate_weight.shape[0]
    experts = exp_local * n_expdev
    tok_rows = tokens.shape[0]
    slot_cap = 4 * tok_rows // experts
    flat_ids = expert_ids.reshape(-1)
    onehot = (flat_ids[:, None] == jnp.arange(experts, dtype=jnp.int32)[None, :]).astype(jnp.int32)
    slots = jnp.sum((jnp.cumsum(onehot, axis=0) - onehot) * onehot, axis=1)
    target = flat_ids * slot_cap + slots
    values = tokens.astype(jnp.float32)
    squares = lax.psum(jnp.sum(values * values, axis=1), "tp")
    factor = lax.rsqrt(squares / D + EPS)
    normed = (values * factor[:, None] * norm_gain.astype(jnp.float32)[None, :]).astype(
        jnp.bfloat16
    )
    rows = jnp.repeat(normed, 2, axis=0)
    buffer = jnp.zeros((experts * slot_cap, normed.shape[1]), jnp.bfloat16).at[target].set(rows)
    buffer = buffer.reshape(n_expdev, exp_local, slot_cap, normed.shape[1])
    arrived = lax.all_to_all(buffer, "ep", split_axis=0, concat_axis=0, tiled=True)
    piece = lax.all_gather(arrived, "tp", axis=3, tiled=True)
    first = jnp.einsum("secd,edf->secf", piece, gate_weight, preferred_element_type=jnp.float32)
    second = jnp.einsum("secd,edf->secf", piece, up_weight, preferred_element_type=jnp.float32)
    hidden = (jax.nn.silu(first) * second).astype(jnp.bfloat16)
    width_local = D // lax.axis_size("tp")
    term = jnp.einsum("secf,efd->dsec", hidden, down_weight, preferred_element_type=jnp.float32)
    summed = lax.psum_scatter(
        term.reshape(lax.axis_size("tp") * width_local, n_expdev * exp_local * slot_cap).astype(
            jnp.bfloat16
        ),
        "tp",
        scatter_dimension=0,
        tiled=True,
    )
    results = summed.reshape(width_local, n_expdev, exp_local, slot_cap)
    results = jnp.transpose(results, (1, 2, 3, 0))
    returned = lax.all_to_all(results, "ep", split_axis=0, concat_axis=0, tiled=True)
    flat_back = returned.reshape(experts * slot_cap, width_local)
    picked = flat_back[target].astype(jnp.float32).reshape(tok_rows, 2, width_local)
    return jnp.sum(picked * gate_share[:, :, None], axis=1).astype(jnp.bfloat16)


def solution(mesh):
    in_specs = (
        P("ep", "tp"),
        P("tp"),
        P("ep", None),
        P("ep", None),
        P("ep", None, "tp"),
        P("ep", None, "tp"),
        P("ep", "tp", None),
    )
    out_specs = P("ep", "tp")
    return jax.shard_map(shards, mesh=mesh, in_specs=in_specs, out_specs=out_specs, check_vma=False)
```

profile of v0, /device:TPU:0, one launch (start us, length us, event | category | flops | bytes accessed | tf_op | source)
XLA Modules:
  0.0 194.9 jit_solution(15358581536983381263)
XLA Ops:
  6.5 0.0 all-gather.2.cloned.1.call-start
  6.5 0.8 copy.14
  7.4 0.1 eq.29
  7.5 0.1 eq.25
  7.6 0.7 broadcast_multiply_fusion
  8.3 1.1 reduce-window.6
  9.5 0.2 slice_reduce_fusion
  9.7 0.1 copy.13
  9.9 0.1 mul.55
  10.0 1.1 fusion.18
  11.1 8.4 %psum.7 = f32[256]{0:T(256)S(1)} all-reduce(f32[256]{0:T(256)S(1)} %fusion.18), channel_id=1, replica_groups=mesh['ep'=8,'tp'=4] {'tp'}, use_global_device_ids=true, to_apply=%region_4.5 | all-reduce | flops 256 | bytes 2048 | tf_op jit(solution)/shard_map/psum | solution.py:23
  19.5 0.7 convert_element_type.38
  20.2 1.1 fusion.20
  21.2 0.3 broadcast_in_dim.5
  21.5 0.2 reshape.107
  21.7 0.1 fusion.24
  21.8 2.7 %scatter_custom_fusion = bf16[1024,512]{1,0:T(8,128)(2,1)S(1)} fusion(s32[512]{0:T(512)S(1)} %bitcast.73, bf16[512,512]{1,0:T(8,128)(2,1)S(1)} %reshape.107, bf16[]{:T(256)} %constant.8.clone.1), kind=kCustom, calls=%fused_computation.24 | custom fusion | bytes 1048578 | tf_op jit(solution)/shard_map/scatter | solution.py:29
  24.6 30.3 %all_to_all.10 = bf16[8,1,128,512]{3,2,1,0:T(8,128)(2,1)} all-to-all(bf16[8,1,128,512]{3,2,1,0:T(8,128)(2,1)S(1)} %bitcast.71), channel_id=1, replica_groups=mesh['ep'=8,'tp'=4] {'ep'}, dimensions={0} | all-to-all | bytes 2097152 | tf_op jit(solution)/shard_map/all_to_all | solution.py:31
  54.9 0.0 all-gather.2.cloned.1.call-update
  54.9 0.0 reduce-scatter.2.cloned.1.call-start
  55.0 33.6 %all-gather.2.cloned.1.call-done = bf16[8,1,128,2048]{3,2,0,1:T(8,128)(2,1)} async-done(((bf16[8,1,128,512]{3,2,0,1:T(8,128)(2,1)}), bf16[8,1,128,2048]{3,2,0,1:T(8,128)(2,1)}) %all-gather.2.cloned.1.call-update) | async-done | bytes 4194320 | tf_op jit(solution)/shard_map/all_gather | solution.py:32
  88.6 0.0 copy-start.1
  88.6 0.0 copy-start.3
  88.6 7.6 %fusion.3 = f32[8,128,1024]{2,1,0:T(8,128)S(1)} fusion(bf16[1,2048,1024]{2,1,0:T(8,128)(2,1)} %param.12, bf16[8,1,128,2048]{3,2,0,1:T(8,128)(2,1)} %all-gather.2.cloned.1.call-done), kind=kOutput, calls=%fused_computation.6 | convolution fusion | flops 4294967296 | bytes 12582912 | tf_op jit(solution)/shard_map/secd,edf->secf/dot_general | solution.py:34
  96.2 0.0 copy-done.1
  96.2 0.0 copy-done.3
  96.2 0.0 copy-start.2
  96.2 5.3 %fusion = bf16[8,1,128,1024]{3,2,0,1:T(8,128)(2,1)S(1)} fusion(f32[8,128,1024]{2,1,0:T(8,128)S(1)} %fusion.3, bf16[1,2048,1024]{2,1,0:T(8,128)(2,1)S(1)} %copy-done.1, bf16[8,1,128,2048]{3,2,0,1:T(8,128)(2,1)S(1)} %copy-done.3), kind=kOutput, calls=%fused_computation.3 | convolution fusion | flops 4301258752 | bytes 14680064 | tf_op jit(solution)/shard_map/secd,edf->secf/dot_general | solution.py:33
  101.6 0.0 copy-done.2
  101.6 6.0 %convert_bitcast_fusion = bf16[2048,1024]{0,1:T(8,128)(2,1)} fusion(bf16[1024,1024]{1,0:T(8,128)(2,1)S(1)} %bitcast.76, bf16[1,1024,2048]{2,1,0:T(8,128)(2,1)S(1)} %copy-done.2), kind=kOutput, calls=%fused_computation.17 | convolution fusion | flops 4297064448 | bytes 10485760 | tf_op jit(solution)/shard_map/secf,efd->dsec/dot_general | solution.py:37
  107.6 0.0 copy-start
  107.6 0.0 reduce-scatter.2.cloned.1.call-update
  107.6 44.6 %reduce-scatter.2.cloned.1.call-done = bf16[512,1024]{0,1:T(8,128)(2,1)} async-done(((bf16[2048,1024]{0,1:T(8,128)(2,1)}), bf16[512,1024]{0,1:T(8,128)(2,1)}) %reduce-scatter.2.cloned.1.call-update) | async-done | bytes 1048592 | tf_op jit(solution)/shard_map/reduce_scatter | solution.py:38
  152.2 5.5 %all-to-all-start.1 = ((bf16[8,1,128,512]{3,2,1,0:T(8,128)(2,1)}), bf16[8,1,128,512]{3,2,1,0:T(8,128)(2,1)S(1)}, u32[]{:S(2)}, u32[]{:S(2)}) async-start(bf16[8,1,128,512]{3,2,1,0:T(8,128)(2,1)} %bitcast.72), calls=%async_computation.2 | async-start | bytes 2097152 | tf_op jit(solution)/shard_map/all_to_all | solution.py:48
  157.7 0.0 copy-done
  157.7 0.1 copy.18
  157.9 25.5 %all-to-all-done.1 = bf16[8,1,128,512]{3,2,1,0:T(8,128)(2,1)S(1)} async-done(((bf16[8,1,128,512]{3,2,1,0:T(8,128)(2,1)}), bf16[8,1,128,512]{3,2,1,0:T(8,128)(2,1)S(1)}, u32[]{:S(2)}, u32[]{:S(2)}) %all-to-all-start.1) | async-done | bytes 1048608 | tf_op jit(solution)/shard_map/all_to_all | solution.py:48
  183.4 2.0 %gather_fusion = bf16[512,512]{1,0:T(8,128)(2,1)S(1)} fusion(bf16[1024,512]{1,0:T(8,128)(2,1)S(1)} %bitcast.69, s32[1024]{0:T(1024)S(1)} %pad_clamp_fusion), kind=kCustom, calls=%fused_computation | custom fusion | bytes 1050624 | tf_op jit(solution)/shard_map/gather | solution.py:50
  185.4 0.7 reshape.94
  186.0 2.1 %multiply_reduce_fusion = bf16[256,512]{1,0:T(8,128)(2,1)} fusion(f32[256,2,512]{2,1,0:T(2,128)S(1)} %reshape.94, f32[256,2]{1,0:T(8,128)S(1)} %copy.18), kind=kLoop, calls=%fused_computation.18 | loop fusion | flops 393216 | bytes 1312768 | tf_op jit(solution)/shard_map/reduce_sum | solution.py:51
  (6 shorter events, 0.1 us)
Async XLA Ops:
  6.5 82.0 %all-gather.2.cloned.1.call-start = ((), (), s32[]{:S(2)}) async-start(), calls=%async_computation.3 | async-start | bytes 5242880 | tf_op jit(solution)/shard_map/all_gather | solution.py:32
  54.9 97.3 %reduce-scatter.2.cloned.1.call-start = ((), (), s32[]{:S(2)}) async-start(), calls=%async_computation.4 | async-start | bytes 5242880 | tf_op jit(solution)/shard_map/reduce_scatter | solution.py:38
  88.6 7.7 %copy-start.1 = (bf16[1,2048,1024]{2,1,0:T(8,128)(2,1)S(1)}, bf16[1,2048,1024]{2,1,0:T(8,128)(2,1)}, u32[]{:S(2)}) copy-start(bf16[1,2048,1024]{2,1,0:T(8,128)(2,1)} %param.11) | copy-start | bytes 12582916
  88.6 7.7 %copy-start.3 = (bf16[8,1,128,2048]{3,2,0,1:T(8,128)(2,1)S(1)}, bf16[8,1,128,2048]{3,2,0,1:T(8,128)(2,1)}, u32[]{:S(2)}) copy-start(bf16[8,1,128,2048]{3,2,0,1:T(8,128)(2,1)} %all-gather.2.cloned.1.call-done) | copy-start | bytes 12582916
  96.2 5.3 %copy-start.2 = (bf16[1,1024,2048]{2,1,0:T(8,128)(2,1)S(1)}, bf16[1,1024,2048]{2,1,0:T(8,128)(2,1)}, u32[]{:S(2)}) copy-start(bf16[1,1024,2048]{2,1,0:T(8,128)(2,1)} %param.13) | copy-start | bytes 12582916
  107.6 50.1 %copy-start = (f32[256,2]{0,1:T(2,128)S(1)}, f32[256,2]{0,1:T(2,128)}, u32[]{:S(2)}) copy-start(f32[256,2]{0,1:T(2,128)} %param.10) | copy-start | bytes 6148
  152.2 31.2 %all-to-all-start.1 = ((bf16[8,1,128,512]{3,2,1,0:T(8,128)(2,1)}), bf16[8,1,128,512]{3,2,1,0:T(8,128)(2,1)S(1)}, u32[]{:S(2)}, u32[]{:S(2)}) async-start(bf16[8,1,128,512]{3,2,1,0:T(8,128)(2,1)} %bitcast.72), calls=%async_computation.2 | async-start | bytes 2097152 | tf_op jit(solution)/shard_map/all_to_all | solution.py:48
Sparse Core Ops, SparseCore 0:
  55.0 33.4 all-gather.1
  107.8 44.3 reduce-scatter.1
where the time goes:
time: 195 us
  waiting for transfers between devices  104 us (53%)
  blocking collectives  38.7 us (20%)
  matrix products  19 us (10%)
  between operations  13.5 us (7%)
  local copies, waits for them, and re-layouts  7.57 us (4%)
  other arithmetic  6.87 us (4%)
  starting transfers between devices  5.56 us (3%)
    reduce_scatter x1, waiting for transfers between devices, shards(): lax.psum_scatter(term.reshape(lax.axis_size('tp') * width_local, n_expdev...  44.6 us
    all_gather x1, waiting for transfers between devices, shards(): piece = lax.all_gather(arrived, 'tp', axis=3, tiled=True)  33.6 us
    all_to_all x1, blocking collectives, shards(): lax.all_to_all(buffer, 'ep', split_axis=0, concat_axis=0, tiled=True)  30.3 us
    all_to_all x1, waiting for transfers between devices, shards(): lax.all_to_all(results, 'ep', split_axis=0, concat_axis=0, tiled=True)  25.5 us
    psum x1, blocking collectives, shards(): squares = lax.psum(jnp.sum(values * values, axis=1), 'tp')  8.37 us
    dot_general x1, matrix products, shards(): jnp.einsum('secd,edf->secf', piece, up_weight, preferred_element_type=jnp...  7.64 us
    dot_general x1, matrix products, shards(): jnp.einsum('secf,efd->dsec', hidden, down_weight, preferred_element_type=...  6.05 us
    all_to_all x1, starting transfers between devices, shards(): lax.all_to_all(results, 'ep', split_axis=0, concat_axis=0, tiled=True)  5.52 us
  transfers between devices with their start and end apart: 3, of which 3 were waited for; matrix products, arithmetic and copies ran while one was open for 0% of the time, Pallas kernels for 0%

commit v1 on v0

--- a/solution.py
+++ b/solution.py
@@ -1,15 +1,22 @@
+import functools
 import jax
 import jax.numpy as jnp
 from jax import lax
+from jax.experimental import pallas as pl
+from jax.experimental.pallas import tpu as pltpu
 from jax.sharding import PartitionSpec as P
 
 D = 2048
 
 
 EPS = 1e-06
-
-
-def shards(tokens, norm_gain, expert_ids, gate_share, gate_weight, up_weight, down_weight):
+MESH = pl.DeviceIdType.MESH
+BF = jnp.bfloat16
+F32 = jnp.float32
+CORES = 2
+
+
+def plain(tokens, norm_gain, expert_ids, gate_share, gate_weight, up_weight, down_weight):
     n_expdev = lax.axis_size("ep")
     exp_local = gate_weight.shape[0]
     experts = exp_local * n_expdev
@@ -51,7 +58,316 @@
     return jnp.sum(picked * gate_share[:, :, None], axis=1).astype(jnp.bfloat16)
 
 
+def fused(
+    n, n_tp, early,
+    tok_ref, gain_ref, ids_ref, share_ref, wg_hbm, wu_hbm, wd_hbm,
+    out_ref,
+    wg, wu, wd, part, near, far, slot_row, share_row, send_a, send_b, xs,
+    hid, own_y, ys, yd, za, zs, zx, rs, ra, mix_hi, mix_lo,
+    w_sem, p_send, p_recv, n_send, n_recv, a_send, a_recv, b_send, b_recv,
+    d_send, d_recv, y_send, y_recv, z_send, z_recv, r_send, r_recv,
+):
+    me = lax.axis_index("ep")
+    tp = lax.axis_index("tp")
+    x, c = tp // CORES, tp % CORES
+    partner = x * CORES + (1 - c)
+    across = (1 - x) * CORES + c
+    diag = (1 - x) * CORES + (1 - c)
+    rows, width = tok_ref.shape
+    cap = send_a.shape[1]
+
+    loads = [
+        pltpu.make_async_copy(wg_hbm.at[0], wg, w_sem.at[0]),
+        pltpu.make_async_copy(wu_hbm.at[0], wu, w_sem.at[1]),
+    ] + [
+        pltpu.make_async_copy(wd_hbm.at[0, :, pl.ds(q * width, width)], wd.at[q], w_sem.at[2 + q])
+        for q in range(n_tp)
+    ]
+    for load in loads:
+        load.start()
+
+    barrier = pltpu.get_barrier_semaphore()
+    for other in (partner, across, diag):
+        pl.semaphore_signal(barrier, inc=1, device_id=(me, other), device_id_type=MESH)
+    for k in range(1, n):
+        pl.semaphore_signal(barrier, inc=1, device_id=((me + k) % n, tp), device_id_type=MESH)
+
+    def remote(src, dst, ssem, rsem, e, t):
+        return pltpu.make_async_remote_copy(
+            src_ref=src, dst_ref=dst, send_sem=ssem, recv_sem=rsem,
+            device_id=(e, t), device_id_type=MESH,
+        )
+
+    def lanes_to_rows(v):
+        return jnp.transpose(v)
+
+    xf = tok_ref[...].astype(F32)
+    sq = xf * xf
+    groups = sq[:, 0:128]
+    for j in range(1, width // 128):
+        groups = groups + sq[:, j * 128:(j + 1) * 128]
+    mine = jnp.sum(lanes_to_rows(groups), axis=0, keepdims=True)
+    part[0] = jnp.broadcast_to(mine, (8, rows))
+
+    pl.semaphore_wait(barrier, 3 + n - 1)
+    p_copies = [
+        remote(part.at[0], part.at[j], p_send.at[j], p_recv.at[j], me, other)
+        for j, other in ((1, partner), (2, across), (3, diag))
+    ]
+    for copy in p_copies:
+        copy.start()
+
+    experts = slot_row.shape[0]
+    expert_of = lax.broadcasted_iota(jnp.int32, (experts, rows), 0)
+    first = expert_of == ids_ref[0:1, :]
+    second = expert_of == ids_ref[1:2, :]
+    named = jnp.where(first | second, 1.0, 0.0)
+    before = (
+        lax.broadcasted_iota(jnp.int32, (rows, rows), 0)
+        < lax.broadcasted_iota(jnp.int32, (rows, rows), 1)
+    )
+    earlier = jnp.dot(
+        named.astype(BF), jnp.where(before, 1.0, 0.0).astype(BF), preferred_element_type=F32
+    )
+    slot_row[...] = jnp.where(named > 0.5, earlier, -1.0)
+    share_row[...] = jnp.where(first, share_ref[0:1, :], 0.0) + jnp.where(
+        second, share_ref[1:2, :], 0.0
+    )
+    slot_of = lax.broadcasted_iota(jnp.int32, (cap, rows), 0).astype(F32)
+
+    def placed(k):
+        e = (me + k) % n
+        return slot_of == jnp.broadcast_to(slot_row[pl.ds(e, 1), :], (cap, rows))
+
+    def place(k):
+        return jnp.where(placed(k), 1.0, 0.0).astype(BF)
+
+    for copy in p_copies:
+        copy.wait_recv()
+    total = part[0] + part[1] + part[2] + part[3]
+    factor = lax.rsqrt(total[0:1, :] / (width * n_tp) + EPS)
+    column = jnp.transpose(jnp.broadcast_to(factor, (128, rows)))
+    column = jnp.concatenate([column] * (width // 128), axis=1)
+    near[...] = (xf * column * gain_ref[...].astype(F32)).astype(BF)
+    n_copy = remote(near, far, n_send, n_recv, me, across)
+    n_copy.start()
+
+    def a_copy(k, e):
+        return remote(send_a.at[k], xs.at[k, c, x], a_send.at[k], a_recv.at[k], e, tp)
+
+    def b_copy(k, e):
+        return remote(send_b.at[k], xs.at[k, c, 1 - x], b_send.at[k], b_recv.at[k], e, tp)
+
+    def send_near(k):
+        send_a[k] = jnp.dot(place(k), near[...], preferred_element_type=F32).astype(BF)
+        a_copy(k, (me + k) % n).start()
+
+    def send_far(k):
+        send_b[k] = jnp.dot(place(k), far[...], preferred_element_type=F32).astype(BF)
+        b_copy(k, (me + k) % n).start()
+
+    @pl.loop(1, early)
+    def _(k):
+        send_near(k)
+
+    xs[0, c, x] = jnp.dot(place(0), near[...], preferred_element_type=F32).astype(BF)
+
+    def weigh(k):
+        e = (me + k) % n
+        weight = jnp.where(
+            placed(k), jnp.broadcast_to(share_row[pl.ds(e, 1), :], (cap, rows)), 0.0
+        )
+        weight = jnp.transpose(weight)
+        high = weight.astype(BF)
+        mix_hi[k] = high
+        mix_lo[k] = (weight - high.astype(F32)).astype(BF)
+
+    n_copy.wait_recv()
+    xs[0, c, 1 - x] = jnp.dot(place(0), far[...], preferred_element_type=F32).astype(BF)
+
+    def d_copy(k):
+        return remote(xs.at[k, c], xs.at[k, c], d_send.at[k], d_recv.at[k], me, partner)
+
+    def d_arrival(k):
+        return remote(xs.at[k, 1 - c], xs.at[k, 1 - c], d_send.at[k], d_recv.at[k], me, partner)
+
+    def y_copy(k):
+        return remote(ys.at[k], yd.at[k], y_send.at[k], y_recv.at[k], me, partner)
+
+    def z_copy(k):
+        return remote(zs.at[k], zx.at[k], z_send.at[k], z_recv.at[k], me, across)
+
+    def r_copy(k):
+        return remote(rs.at[k], ra.at[k], r_send.at[k], r_recv.at[k], (me + n - k) % n, tp)
+
+    @pl.loop(1, early)
+    def _(k):
+        send_far(k)
+
+    @pl.loop(early, n)
+    def _(k):
+        send_near(k)
+        send_far(k)
+
+    @pl.loop(0, n)
+    def _(k):
+        weigh(k)
+
+    for load in loads:
+        load.wait()
+
+    def column_of(q_x, q_c):
+        return wd[q_x * CORES + q_c]
+
+    ff = wg.shape[1]
+    tile = 256 if ff % 256 == 0 else 128
+
+    @pl.loop(0, n + 2)
+    def _(k):
+        @pl.when((k >= 1) & (k < n))
+        def _():
+            a_copy(k, me).wait_recv()
+            b_copy(k, me).wait_recv()
+
+        @pl.when(k < n)
+        def _():
+            d_copy(k).start()
+
+        @pl.when((k >= 1) & (k <= n))
+        def _():
+            j = k - 1
+            y_copy(j).wait_recv()
+            zs[j] = (own_y[j, 1] + yd[j, 1].astype(F32)).astype(BF)
+            z_copy(j).start()
+            za[j] = own_y[j, 0] + yd[j, 0].astype(F32)
+
+        @pl.when(k < n)
+        def _():
+            d_arrival(k).wait_recv()
+            block = jnp.concatenate(
+                [xs[k, q % CORES, q // CORES] for q in range(n_tp)], axis=1
+            )
+            for f in range(0, ff, tile):
+                gate = jnp.dot(block, wg[:, f:f + tile], preferred_element_type=F32)
+                up = jnp.dot(block, wu[:, f:f + tile], preferred_element_type=F32)
+                hid[:, f:f + tile] = (gate / (1.0 + jnp.exp(-gate)) * up).astype(BF)
+            hidden = hid[...]
+            for i, q_x in enumerate((x, 1 - x)):
+                ys[k, i] = jnp.dot(
+                    hidden, column_of(q_x, 1 - c), preferred_element_type=F32
+                ).astype(BF)
+            y_copy(k).start()
+            for i, q_x in enumerate((x, 1 - x)):
+                own_y[k, i] = jnp.dot(hidden, column_of(q_x, c), preferred_element_type=F32)
+
+        @pl.when(k >= 2)
+        def _():
+            j = k - 2
+            z_copy(j).wait_recv()
+            result = (za[j] + zx[j].astype(F32)).astype(BF)
+
+            @pl.when(j == 0)
+            def _():
+                ra[0] = result
+
+            @pl.when(j > 0)
+            def _():
+                rs[j] = result
+                r_copy(j).start()
+
+    def mixed(k):
+        back = ra[k]
+        return jnp.dot(mix_hi[k], back, preferred_element_type=F32) + jnp.dot(
+            mix_lo[k], back, preferred_element_type=F32
+        )
+
+    total = mixed(0)
+    for k in range(1, n):
+        r_copy(k).wait_recv()
+        total = total + mixed(k)
+    out_ref[...] = total.astype(BF)
+
+    for copy in p_copies:
+        copy.wait_send()
+    n_copy.wait_send()
+    for k in range(n):
+        d_copy(k).wait_send()
+        y_copy(k).wait_send()
+        z_copy(k).wait_send()
+        if k:
+            a_copy(k, me).wait_send()
+            b_copy(k, me).wait_send()
+            r_copy(k).wait_send()
+
+
+def routed(n, n_tp, tokens, norm_gain, expert_ids, gate_share, gate_weight, up_weight, down_weight):
+    rows, width = tokens.shape
+    experts = n * gate_weight.shape[0]
+    cap = 4 * rows // experts
+    depth, ff = gate_weight.shape[1:]
+    vmem = pl.BlockSpec(memory_space=pltpu.VMEM)
+    hbm = pl.BlockSpec(memory_space=pltpu.HBM)
+    dma = pltpu.SemaphoreType.DMA
+    return pl.pallas_call(
+        functools.partial(fused, n, n_tp, (n + 1) // 2),
+        out_shape=jax.ShapeDtypeStruct((rows, width), BF),
+        in_specs=[vmem] * 4 + [hbm] * 3,
+        out_specs=vmem,
+        scratch_shapes=[
+            pltpu.VMEM((depth, ff), BF),
+            pltpu.VMEM((depth, ff), BF),
+            pltpu.VMEM((n_tp, ff, width), BF),
+            pltpu.VMEM((4, 8, rows), F32),
+            pltpu.VMEM((rows, width), BF),
+            pltpu.VMEM((rows, width), BF),
+            pltpu.VMEM((experts, rows), F32),
+            pltpu.VMEM((experts, rows), F32),
+            pltpu.VMEM((n, cap, width), BF),
+            pltpu.VMEM((n, cap, width), BF),
+            pltpu.VMEM((n, CORES, n_tp // CORES, cap, width), BF),
+            pltpu.VMEM((cap, ff), BF),
+            pltpu.VMEM((n, 2, cap, width), F32),
+            pltpu.VMEM((n, 2, cap, width), BF),
+            pltpu.VMEM((n, 2, cap, width), BF),
+            pltpu.VMEM((n, cap, width), F32),
+            pltpu.VMEM((n, cap, width), BF),
+            pltpu.VMEM((n, cap, width), BF),
+            pltpu.VMEM((n, cap, width), BF),
+            pltpu.VMEM((n, cap, width), BF),
+            pltpu.VMEM((n, rows, cap), BF),
+            pltpu.VMEM((n, rows, cap), BF),
+            dma((2 + n_tp,)),
+            dma((4,)), dma((4,)),
+            dma, dma,
+            dma((n,)), dma((n,)),
+            dma((n,)), dma((n,)),
+            dma((n,)), dma((n,)),
+            dma((n,)), dma((n,)),
+            dma((n,)), dma((n,)),
+            dma((n,)), dma((n,)),
+        ],
+        compiler_params=pltpu.CompilerParams(
+            collective_id=0, has_side_effects=True, vmem_limit_bytes=56 * 1024 * 1024
+        ),
+    )(
+        tokens, norm_gain.reshape(1, width), expert_ids.T, gate_share.T,
+        gate_weight, up_weight, down_weight,
+    )
+
+
+def shards(n, n_tp, *args):
+    tokens, gate_weight = args[0], args[4]
+    rows, width = tokens.shape
+    cap = 4 * rows // (n * gate_weight.shape[0])
+    fits = (
+        n_tp == 2 * CORES and gate_weight.shape[0] == 1 and rows % 128 == 0
+        and width % 128 == 0 and gate_weight.shape[2] % 128 == 0 and cap % 128 == 0
+    )
+    return routed(n, n_tp, *args) if fits else plain(*args)
+
+
 def solution(mesh):
+    body = functools.partial(shards, mesh.shape["ep"], mesh.shape["tp"])
     in_specs = (
         P("ep", "tp"),
         P("tp"),
@@ -62,4 +378,4 @@
         P("ep", "tp", None),
     )
     out_specs = P("ep", "tp")
-    return jax.shard_map(shards, mesh=mesh, in_specs=in_specs, out_specs=out_specs, check_vma=False)
+    return jax.shard_map(body, mesh=mesh, in_specs=in_specs, out_specs=out_specs, check_vma=False)

time: 195 us -> 99.1 us (0.51)
  waiting for transfers between devices: 104 us -> 0 us
  Pallas kernels: 0 us -> 96 us
  blocking collectives: 38.7 us -> 0 us
  matrix products: 19 us -> 0 us
  between operations: 13.5 us -> 0.01 us
  other arithmetic: 6.87 us -> 0 us
  starting transfers between devices: 5.56 us -> 0 us
  local copies, waits for them, and re-layouts: 7.57 us -> 2.93 us
    pallas_call x0 -> x1, Pallas kernels: none -> 96 us  [routed(): pl.pallas_call(functools.partial(fused, n, n_tp, (n + 1) // 2), out_shape...]
    reduce_scatter x1 -> x0, waiting for transfers between devices: 44.6 us -> none  [shards(): lax.psum_scatter(term.reshape(lax.axis_size('tp') * width_local, n_expdev...]
    all_gather x1 -> x0, waiting for transfers between devices: 33.6 us -> none  [shards(): piece = lax.all_gather(arrived, 'tp', axis=3, tiled=True)]
    all_to_all x1 -> x0, blocking collectives: 30.3 us -> none  [shards(): lax.all_to_all(buffer, 'ep', split_axis=0, concat_axis=0, tiled=True)]
    all_to_all x1 -> x0, waiting for transfers between devices: 25.5 us -> none  [shards(): lax.all_to_all(results, 'ep', split_axis=0, concat_axis=0, tiled=True)]
    dot_general x3 -> x0, matrix products: 19 us -> none  [the longest x1 7.64 us: shards(): jnp.einsum('secd,edf->secf', piece, up_weight, preferred_element_type=jnp...]
    psum x1 -> x0, blocking collectives: 8.37 us -> none  [shards(): squares = lax.psum(jnp.sum(values * values, axis=1), 'tp')]
    all_to_all x1 -> x0, starting transfers between devices: 5.52 us -> none  [shards(): lax.all_to_all(results, 'ep', split_axis=0, concat_axis=0, tiled=True)]
  transfers between devices with their start and end apart: 3 -> 0, of which waited for: 3 -> 0; matrix products, arithmetic and copies ran while one was open for 0% -> 0% of each run, Pallas kernels for 0% -> 0%
where the time goes in v1:
time: 99.1 us; the launch traced here: 98.9 us
  Pallas kernels  96 us (97%)
  local copies, waits for them, and re-layouts  2.93 us (3%)
    pallas_call x1, Pallas kernels, routed(): pl.pallas_call(functools.partial(fused, n, n_tp, (n + 1) // 2), out_shape...  96 us

profile of v1, /device:TPU:0, one launch (start us, length us, event | category | flops | bytes accessed | tf_op | source)
XLA Modules:
  0.0 98.9 jit_solution(17069328617901849151)
XLA Ops:
  0.0 1.3 %reshape.3.gain_ref = bf16[1,512]{1,0:T(2,128)(2,1)} reshape(bf16[512]{0:T(512)(128)(2,1)} %param.8) | data formatting | bytes 2048 | tf_op jit(solution)/shard_map/reshape | solution.py:353
  1.3 96.0 %shard_map.73 = bf16[256,512]{1,0:T(8,128)(2,1)} custom-call(bf16[256,512]{1,0:T(8,128)(2,1)} %tok_ref.1, bf16[1,512]{1,0:T(2,128)(2,1)} %reshape.3.gain_ref, s32[2,256]{1,0:T(2,128)} %bitcast.2, f32[2,256]{1,0:T(2,128)} %bitcast.3, bf16[1,2048,1024]{2,1,0:T(8,128)(2,1)} %wg_hbm.1, bf16[1,2048,1024]{2,1,0:T(8,128)(2,1)} %wu_hbm.1, bf16[1,1024,2048]{2,1,0:T(8,128)(2,1)} %wd_hbm.1), custom_call_target="tpu_custom_call" | custom-call | tf_op jit(solution)/shard_map/pallas_call | solution.py:311
  97.3 1.7 %copy.9 = bf16[256,512]{1,0:T(8,128)(2,1)} copy(bf16[256,512]{1,0:T(8,128)(2,1)} %shard_map.73) | data formatting | bytes 524288

commit v2 on v1

--- a/solution.py
+++ b/solution.py
@@ -59,13 +59,13 @@
 
 
 def fused(
-    n, n_tp, early,
+    n, n_tp, steps,
     tok_ref, gain_ref, ids_ref, share_ref, wg_hbm, wu_hbm, wd_hbm,
     out_ref,
     wg, wu, wd, part, near, far, slot_row, share_row, send_a, send_b, xs,
     hid, own_y, ys, yd, za, zs, zx, rs, ra, mix_hi, mix_lo,
     w_sem, p_send, p_recv, n_send, n_recv, a_send, a_recv, b_send, b_recv,
-    d_send, d_recv, y_send, y_recv, z_send, z_recv, r_send, r_recv,
+    f_send, f_recv, d_send, d_recv, e_send, e_recv, y_send, y_recv, z_send, z_recv, r_send, r_recv,
 ):
     me = lax.axis_index("ep")
     tp = lax.axis_index("tp")
@@ -75,6 +75,14 @@
     diag = (1 - x) * CORES + (1 - c)
     rows, width = tok_ref.shape
     cap = send_a.shape[1]
+    half = n // 2
+
+    def peer(k):
+        found, bit = 0, 1
+        while bit < n:
+            found = found + (me // bit + k // bit) % 2 * bit
+            bit *= 2
+        return found
 
     loads = [
         pltpu.make_async_copy(wg_hbm.at[0], wg, w_sem.at[0]),
@@ -90,7 +98,7 @@
     for other in (partner, across, diag):
         pl.semaphore_signal(barrier, inc=1, device_id=(me, other), device_id_type=MESH)
     for k in range(1, n):
-        pl.semaphore_signal(barrier, inc=1, device_id=((me + k) % n, tp), device_id_type=MESH)
+        pl.semaphore_signal(barrier, inc=1, device_id=(peer(k), tp), device_id_type=MESH)
 
     def remote(src, dst, ssem, rsem, e, t):
         return pltpu.make_async_remote_copy(
@@ -136,7 +144,7 @@
     slot_of = lax.broadcasted_iota(jnp.int32, (cap, rows), 0).astype(F32)
 
     def placed(k):
-        e = (me + k) % n
+        e = peer(k)
         return slot_of == jnp.broadcast_to(slot_row[pl.ds(e, 1), :], (cap, rows))
 
     def place(k):
@@ -160,20 +168,22 @@
 
     def send_near(k):
         send_a[k] = jnp.dot(place(k), near[...], preferred_element_type=F32).astype(BF)
-        a_copy(k, (me + k) % n).start()
+        a_copy(k, peer(k)).start()
 
     def send_far(k):
         send_b[k] = jnp.dot(place(k), far[...], preferred_element_type=F32).astype(BF)
-        b_copy(k, (me + k) % n).start()
-
-    @pl.loop(1, early)
-    def _(k):
+        b_copy(k, peer(k)).start()
+
+    first_far = half + half // 2
+    for k in range(half, first_far):
         send_near(k)
+    for k in range(1, half):
+        send_near(k)
 
     xs[0, c, x] = jnp.dot(place(0), near[...], preferred_element_type=F32).astype(BF)
 
     def weigh(k):
-        e = (me + k) % n
+        e = peer(k)
         weight = jnp.where(
             placed(k), jnp.broadcast_to(share_row[pl.ds(e, 1), :], (cap, rows)), 0.0
         )
@@ -185,11 +195,26 @@
     n_copy.wait_recv()
     xs[0, c, 1 - x] = jnp.dot(place(0), far[...], preferred_element_type=F32).astype(BF)
 
-    def d_copy(k):
-        return remote(xs.at[k, c], xs.at[k, c], d_send.at[k], d_recv.at[k], me, partner)
-
-    def d_arrival(k):
-        return remote(xs.at[k, 1 - c], xs.at[k, 1 - c], d_send.at[k], d_recv.at[k], me, partner)
+    for i in range(max(half - 1, n - first_far)):
+        if i + 1 < half:
+            send_far(i + 1)
+        if first_far + i < n:
+            send_near(first_far + i)
+
+    def f_copy(k):
+        return remote(xs.at[k, c, x], xs.at[k, c, x], f_send.at[k], f_recv.at[k], me, across)
+
+    def f_arrival(k):
+        there = xs.at[k, c, 1 - x]
+        return remote(there, there, f_send.at[k], f_recv.at[k], me, across)
+
+    def d_copy(k, core):
+        ref = xs.at[k, core] if k < half else xs.at[k, core, x]
+        return remote(ref, ref, d_send.at[k], d_recv.at[k], me, partner)
+
+    def e_copy(k, core):
+        ref = xs.at[k, core, 1 - x]
+        return remote(ref, ref, e_send.at[k], e_recv.at[k], me, partner)
 
     def y_copy(k):
         return remote(ys.at[k], yd.at[k], y_send.at[k], y_recv.at[k], me, partner)
@@ -198,16 +223,40 @@
         return remote(zs.at[k], zx.at[k], z_send.at[k], z_recv.at[k], me, across)
 
     def r_copy(k):
-        return remote(rs.at[k], ra.at[k], r_send.at[k], r_recv.at[k], (me + n - k) % n, tp)
-
-    @pl.loop(1, early)
-    def _(k):
-        send_far(k)
-
-    @pl.loop(early, n)
-    def _(k):
-        send_near(k)
-        send_far(k)
+        return remote(rs.at[k], ra.at[k], r_send.at[k], r_recv.at[k], peer(k), tp)
+
+    def arrive(ks):
+        for k in ks:
+            if k:
+                a_copy(k, me).wait_recv()
+            if k >= half:
+                f_copy(k).start()
+            elif k:
+                b_copy(k, me).wait_recv()
+            d_copy(k, c).start()
+
+    def pair(ks):
+        for k in ks:
+            y_copy(k).wait_recv()
+            zs[k] = (own_y[k, 1] + yd[k, 1].astype(F32)).astype(BF)
+            z_copy(k).start()
+        for k in ks:
+            za[k] = own_y[k, 0] + yd[k, 0].astype(F32)
+
+    def give(ks):
+        for k in ks:
+            z_copy(k).wait_recv()
+            result = (za[k] + zx[k].astype(F32)).astype(BF)
+            if k:
+                rs[k] = result
+                r_copy(k).start()
+            else:
+                ra[0] = result
+
+    ff = wg.shape[1]
+    tile = 256 if ff % 256 == 0 else 128
+
+    arrive(steps[0])
 
     @pl.loop(0, n)
     def _(k):
@@ -216,64 +265,47 @@
     for load in loads:
         load.wait()
 
-    def column_of(q_x, q_c):
-        return wd[q_x * CORES + q_c]
-
-    ff = wg.shape[1]
-    tile = 256 if ff % 256 == 0 else 128
-
-    @pl.loop(0, n + 2)
-    def _(k):
-        @pl.when((k >= 1) & (k < n))
-        def _():
-            a_copy(k, me).wait_recv()
-            b_copy(k, me).wait_recv()
-
-        @pl.when(k < n)
-        def _():
-            d_copy(k).start()
-
-        @pl.when((k >= 1) & (k <= n))
-        def _():
-            j = k - 1
-            y_copy(j).wait_recv()
-            zs[j] = (own_y[j, 1] + yd[j, 1].astype(F32)).astype(BF)
-            z_copy(j).start()
-            za[j] = own_y[j, 0] + yd[j, 0].astype(F32)
-
-        @pl.when(k < n)
-        def _():
-            d_arrival(k).wait_recv()
-            block = jnp.concatenate(
-                [xs[k, q % CORES, q // CORES] for q in range(n_tp)], axis=1
-            )
-            for f in range(0, ff, tile):
-                gate = jnp.dot(block, wg[:, f:f + tile], preferred_element_type=F32)
-                up = jnp.dot(block, wu[:, f:f + tile], preferred_element_type=F32)
-                hid[:, f:f + tile] = (gate / (1.0 + jnp.exp(-gate)) * up).astype(BF)
-            hidden = hid[...]
-            for i, q_x in enumerate((x, 1 - x)):
-                ys[k, i] = jnp.dot(
-                    hidden, column_of(q_x, 1 - c), preferred_element_type=F32
-                ).astype(BF)
+    for step, ks in enumerate(steps):
+        for k in ks:
+            if k >= half:
+                f_arrival(k).wait_recv()
+                e_copy(k, c).start()
+        if step >= 1:
+            pair(steps[step - 1])
+        if step >= 2:
+            give(steps[step - 2])
+        for k in ks:
+            d_copy(k, 1 - c).wait_recv()
+            if k >= half:
+                e_copy(k, 1 - c).wait_recv()
+        block = jnp.concatenate(
+            [
+                jnp.concatenate([xs[k, q % CORES, q // CORES] for q in range(n_tp)], axis=1)
+                for k in ks
+            ],
+            axis=0,
+        )
+        held = cap * len(ks)
+        for f in range(0, ff, tile):
+            gate = jnp.dot(block, wg[:, f:f + tile], preferred_element_type=F32)
+            up = jnp.dot(block, wu[:, f:f + tile], preferred_element_type=F32)
+            hid[0:held, f:f + tile] = (gate / (1.0 + jnp.exp(-gate)) * up).astype(BF)
+        if step + 1 < len(steps):
+            arrive(steps[step + 1])
+        hidden = hid[0:held, :]
+        for i, q_x in enumerate((x, 1 - x)):
+            y = jnp.dot(hidden, wd[q_x * CORES + 1 - c], preferred_element_type=F32).astype(BF)
+            for m, k in enumerate(ks):
+                ys[k, i] = y[m * cap:(m + 1) * cap]
+        for k in ks:
             y_copy(k).start()
-            for i, q_x in enumerate((x, 1 - x)):
-                own_y[k, i] = jnp.dot(hidden, column_of(q_x, c), preferred_element_type=F32)
-
-        @pl.when(k >= 2)
-        def _():
-            j = k - 2
-            z_copy(j).wait_recv()
-            result = (za[j] + zx[j].astype(F32)).astype(BF)
-
-            @pl.when(j == 0)
-            def _():
-                ra[0] = result
-
-            @pl.when(j > 0)
-            def _():
-                rs[j] = result
-                r_copy(j).start()
+        for i, q_x in enumerate((x, 1 - x)):
+            y = jnp.dot(hidden, wd[q_x * CORES + c], preferred_element_type=F32)
+            for m, k in enumerate(ks):
+                own_y[k, i] = y[m * cap:(m + 1) * cap]
+    pair(steps[-1])
+    for ks in steps[-2:]:
+        give(ks)
 
     def mixed(k):
         back = ra[k]
@@ -282,7 +314,7 @@
         )
 
     total = mixed(0)
-    for k in range(1, n):
+    for k in [k for ks in steps for k in ks if k]:
         r_copy(k).wait_recv()
         total = total + mixed(k)
     out_ref[...] = total.astype(BF)
@@ -291,13 +323,23 @@
         copy.wait_send()
     n_copy.wait_send()
     for k in range(n):
-        d_copy(k).wait_send()
+        d_copy(k, c).wait_send()
         y_copy(k).wait_send()
         z_copy(k).wait_send()
         if k:
             a_copy(k, me).wait_send()
+            r_copy(k).wait_send()
+        if 0 < k < half:
             b_copy(k, me).wait_send()
-            r_copy(k).wait_send()
+        if k >= half:
+            f_copy(k).wait_send()
+            e_copy(k, c).wait_send()
+
+
+def order(n):
+    half, quarter = n // 2, n // 4
+    starts = (0, half, quarter, half + quarter)
+    return [tuple(range(i, i + 2)) for s in starts for i in range(s, s + quarter, 2)]
 
 
 def routed(n, n_tp, tokens, norm_gain, expert_ids, gate_share, gate_weight, up_weight, down_weight):
@@ -309,7 +351,7 @@
     hbm = pl.BlockSpec(memory_space=pltpu.HBM)
     dma = pltpu.SemaphoreType.DMA
     return pl.pallas_call(
-        functools.partial(fused, n, n_tp, (n + 1) // 2),
+        functools.partial(fused, n, n_tp, order(n)),
         out_shape=jax.ShapeDtypeStruct((rows, width), BF),
         in_specs=[vmem] * 4 + [hbm] * 3,
         out_specs=vmem,
@@ -325,7 +367,7 @@
             pltpu.VMEM((n, cap, width), BF),
             pltpu.VMEM((n, cap, width), BF),
             pltpu.VMEM((n, CORES, n_tp // CORES, cap, width), BF),
-            pltpu.VMEM((cap, ff), BF),
+            pltpu.VMEM((2 * cap, ff), BF),
             pltpu.VMEM((n, 2, cap, width), F32),
             pltpu.VMEM((n, 2, cap, width), BF),
             pltpu.VMEM((n, 2, cap, width), BF),
@@ -339,6 +381,8 @@
             dma((2 + n_tp,)),
             dma((4,)), dma((4,)),
             dma, dma,
+            dma((n,)), dma((n,)),
+            dma((n,)), dma((n,)),
             dma((n,)), dma((n,)),
             dma((n,)), dma((n,)),
             dma((n,)), dma((n,)),
@@ -360,7 +404,7 @@
     rows, width = tokens.shape
     cap = 4 * rows // (n * gate_weight.shape[0])
     fits = (
-        n_tp == 2 * CORES and gate_weight.shape[0] == 1 and rows % 128 == 0
+        n_tp == 2 * CORES and n >= 8 and n & (n - 1) == 0 and gate_weight.shape[0] == 1 and rows % 128 == 0
         and width % 128 == 0 and gate_weight.shape[2] % 128 == 0 and cap % 128 == 0
     )
     return routed(n, n_tp, *args) if fits else plain(*args)

time: 99.1 us -> 83.1 us (0.84)
  Pallas kernels: 96 us -> 79.9 us
    pallas_call x1, Pallas kernels: 96 us -> 79.9 us  [routed(): pl.pallas_call(functools.partial(fused, n, n_tp, order(n)), out_shape=jax...]
where the time goes in v2:
time: 83.1 us; the launch traced here: 82.8 us
  Pallas kernels  79.9 us (96%)
  local copies, waits for them, and re-layouts  2.93 us (4%)
    pallas_call x1, Pallas kernels, routed(): pl.pallas_call(functools.partial(fused, n, n_tp, order(n)), out_shape=jax...  79.9 us
    unnamed x1, local copies, waits for them, and re-layouts  1.67 us

profile of v2, /device:TPU:0, one launch (start us, length us, event | category | flops | bytes accessed | tf_op | source)
XLA Modules:
  0.0 82.8 jit_solution(1565360088954914010)
XLA Ops:
  0.0 1.3 %reshape.3.gain_ref = bf16[1,512]{1,0:T(2,128)(2,1)} reshape(bf16[512]{0:T(512)(128)(2,1)} %param.8) | data formatting | bytes 2048 | tf_op jit(solution)/shard_map/reshape | solution.py:397
  1.3 79.9 %shard_map.73 = bf16[256,512]{1,0:T(8,128)(2,1)} custom-call(bf16[256,512]{1,0:T(8,128)(2,1)} %tok_ref.1, bf16[1,512]{1,0:T(2,128)(2,1)} %reshape.3.gain_ref, s32[2,256]{1,0:T(2,128)} %bitcast.2, f32[2,256]{1,0:T(2,128)} %bitcast.3, bf16[1,2048,1024]{2,1,0:T(8,128)(2,1)} %wg_hbm.1, bf16[1,2048,1024]{2,1,0:T(8,128)(2,1)} %wu_hbm.1, bf16[1,1024,2048]{2,1,0:T(8,128)(2,1)} %wd_hbm.1), custom_call_target="tpu_custom_call" | custom-call | tf_op jit(solution)/shard_map/pallas_call | solution.py:353
  81.2 1.7 %copy.9 = bf16[256,512]{1,0:T(8,128)(2,1)} copy(bf16[256,512]{1,0:T(8,128)(2,1)} %shard_map.73) | data formatting | bytes 524288
